TPU v7x, 32 devices: a whole 2x2x4 slice. The times are simulated.
32 devices in a mesh: sp: 8 (over z, y), tp: 4 (over x, core).
Axes of the slice: x: 2, y: 2, z: 4, core: 2. Of those that a mesh axis runs over, the one named last changes fastest.
Arguments:
- residual: bfloat16 [2048, 2048], P('sp'), may hold values from -6 to 6
- queries: bfloat16 [2048, 8, 2, 128], P('sp', 'tp'), may hold values from -100 to 100
- key_rows: bfloat16 [2048, 8, 2, 128], P('sp', 'tp'), may hold values from -6 to 6
- values: bfloat16 [2048, 8, 256], P('sp', 'tp'), may hold values from -6 to 6
- lambda_head: float32 [8], P('tp'), may hold values from 0.3 to 0.8
- sub_gain: float32 [256], replicated, may hold values from 0.1 to 1.9
- w_out: bfloat16 [2048, 2048], P('tp'), may hold values from -0.125 to 0.125
- norm_gain: float32 [2048], replicated, may hold values from 0.1 to 1.9
- w_gate: bfloat16 [2048, 5632], P('sp', 'tp'), may hold values from -0.125 to 0.125
- w_up: bfloat16 [2048, 5632], P('sp', 'tp'), may hold values from -0.125 to 0.125
- conv_gate: float32 [3, 5632], P(None, 'tp'), may hold values from -3 to 3
- conv_up: float32 [3, 5632], P(None, 'tp'), may hold values from -3 to 3
- w_down: bfloat16 [5632, 2048], P('tp'), may hold values from -0.078125 to 0.078125
Outputs:
- layer_out: bfloat16 [2048, 2048], P(('sp', 'tp'))
All inputs are finite; a program needn't handle non-finite values.
Results may differ from a plain program's by a relative error of at most 0.017.
Values may be sent and summed in bfloat16 or wider, within the bound.
A program may use at most 192 MiB of HBM per device.

v0:
```python
import math

import jax
import jax.numpy as jnp
from jax import lax
from jax.sharding import PartitionSpec as P

epsilon = 1e-06
lambda_init = 0.8 - 0.6 * math.exp(-0.3)


def from_behind(block, axis, distance):
    devices = range(lax.axis_size(axis))
    route = [(i - distance, i) for i in devices if i - distance in devices]
    return lax.ppermute(block, axis, route)


def row_norm(middle, norm_gain):
    row_square = jnp.mean(middle * middle, axis=-1, keepdims=True)
    return (middle * lax.rsqrt(row_square + epsilon) * norm_gain).astype(jnp.bfloat16)


def causal_mix(rows_in, prior_rows, taps):
    padded_rows = jnp.concatenate([prior_rows, rows_in], 0).astype(jnp.float32)
    return taps[0] * padded_rows[:-2] + taps[1] * padded_rows[1:-1] + taps[2] * padded_rows[2:]


def local(
    residual,
    queries,
    key_rows,
    values,
    lambda_head,
    sub_gain,
    w_out,
    norm_gain,
    w_gate,
    w_up,
    conv_gate,
    conv_up,
    w_down,
):
    tok_rows = queries.shape[0]
    head_count = queries.shape[1]
    val_width = values.shape[2]
    score_scale = 1.0 / math.sqrt(queries.shape[3])
    query_pos = lax.axis_index("sp") * tok_rows + jnp.arange(tok_rows, dtype=jnp.int32)
    run_max = jnp.full((head_count, 2, tok_rows), -1e30, jnp.float32)
    key_part = lax.all_gather(key_rows, "sp", axis=0, tiled=True)
    val_part = lax.all_gather(values, "sp", axis=0, tiled=True)
    key_pos = jnp.arange(key_part.shape[0], dtype=jnp.int32)
    causal_mask = key_pos[None, :] <= query_pos[:, None]
    scores = (
        jnp.einsum("qhcd,khcd->hcqk", queries, key_part, preferred_element_type=jnp.float32)
        * score_scale
    )
    scores = jnp.where(causal_mask, scores, -1e30)
    new_max = jnp.maximum(run_max, jnp.max(scores, axis=-1))
    weights = jnp.where(causal_mask, jnp.exp(scores - new_max[..., None]), 0.0)
    run_sum = jnp.sum(weights, axis=-1)
    run_acc = jnp.einsum(
        "hcqk,khe->hcqe", weights.astype(jnp.bfloat16), val_part, preferred_element_type=jnp.float32
    )
    run_max, run_sum, run_acc = (new_max, run_sum, run_acc)
    blended = run_acc / run_sum[..., None]
    attended = blended[:, 0] - lambda_head[:, None, None] * blended[:, 1]
    mean_square = jnp.mean(attended * attended, axis=-1, keepdims=True)
    normed = (attended * lax.rsqrt(mean_square + epsilon) * sub_gain * (1.0 - lambda_init)).astype(
        jnp.bfloat16
    )
    w_heads = w_out.reshape(head_count, val_width, w_out.shape[1])
    part_rows = tok_rows // lax.axis_size("tp")
    own_start = lax.axis_index("tp") * part_rows
    projected = lax.psum(
        jnp.einsum("hqe,hed->qd", normed, w_heads, preferred_element_type=jnp.float32).astype(
            jnp.bfloat16
        ),
        "tp",
    ).astype(jnp.float32)
    middle = residual.astype(jnp.float32) + projected
    gathered = row_norm(middle, norm_gain)
    middle_own = lax.dynamic_slice_in_dim(middle, own_start, part_rows, 0)
    gate_pre = jnp.dot(
        gathered,
        lax.all_gather(w_gate, "sp", axis=0, tiled=True),
        preferred_element_type=jnp.float32,
    )
    up_pre = jnp.dot(
        gathered, lax.all_gather(w_up, "sp", axis=0, tiled=True), preferred_element_type=jnp.float32
    )
    gate_pre = gate_pre.astype(jnp.bfloat16)
    up_pre = up_pre.astype(jnp.bfloat16)
    prior_gate, prior_up = from_behind((gate_pre[-2:], up_pre[-2:]), "sp", 1)
    gate_mixed = causal_mix(gate_pre, prior_gate, conv_gate)
    up_mixed = causal_mix(up_pre, prior_up, conv_up)
    hidden = (jax.nn.silu(gate_mixed) * up_mixed).astype(jnp.bfloat16)
    lowered = lax.psum_scatter(
        jnp.dot(hidden, w_down, preferred_element_type=jnp.float32).astype(jnp.bfloat16),
        "tp",
        scatter_dimension=0,
        tiled=True,
    ).astype(jnp.float32)
    return (middle_own + lowered).astype(jnp.bfloat16)


def solution(mesh):
    placed = (
        P("sp", None),
        P("sp", "tp", None, None),
        P("sp", "tp", None, None),
        P("sp", "tp", None),
        P("tp"),
        P(),
        P("tp", None),
        P(),
        P("sp", "tp"),
        P("sp", "tp"),
        P(None, "tp"),
        P(None, "tp"),
        P("tp", None),
    )
    return jax.shard_map(
        local, mesh=mesh, in_specs=placed, out_specs=P(("sp", "tp"), None), check_vma=False
    )
```

profile of v0, /device:TPU:31, one launch (start us, length us, event | category | flops | bytes accessed | tf_op | source)
XLA Modules:
  0.0 388.9 jit_solution(5965651363115972954)
XLA Ops:
  6.5 0.0 copy-start
  6.5 0.0 copy-start.5
  6.5 0.0 all-gather.5.cloned.1.call-start
  6.5 1.9 copy.14
  8.4 0.0 all-gather.5.cloned.1.call-update
  8.4 0.0 all-gather.7.cloned.1.call-start
  8.5 1.8 copy.16
  10.3 0.0 all-gather.7.cloned.1.call-update
  10.3 0.0 all-reduce.2.cloned.1.call-start
  10.4 0.4 iota_compare_fusion
  10.8 45.8 %all-gather.5.cloned.1.call-done = bf16[2048,2,2,128]{3,0,2,1:T(8,128)(2,1)} async-done(((bf16[256,2,2,128]{3,0,2,1:T(8,128)(2,1)}), bf16[2048,2,2,128]{3,0,2,1:T(8,128)(2,1)}) %all-gather.5.cloned.1.call-update) | async-done | bytes 2097168 | tf_op jit(solution)/shard_map/all_gather | solution.py:49
  56.6 0.0 copy-done.5
  56.6 3.4 fusion
  60.0 0.0 copy-start.1
  60.0 3.2 copy-done.1
  63.2 2.5 fusion.1
  65.7 0.0 copy-start.8
  65.7 0.0 copy-start.9
  65.8 41.9 %all-gather.7.cloned.1.call-done = bf16[2048,2,256]{0,2,1:T(8,128)(2,1)} async-done(((bf16[256,2,256]{0,2,1:T(8,128)(2,1)}), bf16[2048,2,256]{0,2,1:T(8,128)(2,1)}) %all-gather.7.cloned.1.call-update) | async-done | bytes 2097168 | tf_op jit(solution)/shard_map/all_gather | solution.py:50
  107.7 5.8 %fusion.14 = f32[2,2,256,256]{2,3,1,0:T(8,128)S(1)} fusion(bf16[2048,2,256]{0,2,1:T(8,128)(2,1)} %all-gather.7.cloned.1.call-done, f32[2,2,256,2048]{3,2,1,0:T(8,128)} %copy-done.1, f32[2,2,256]{2,1,0:T(2,128)S(1)} %broadcast_maximum_fusion, pred[256,2048]{1,0:T(8,128)(4,1)S(1)} %iota_compare_fusion, f32[2,2,256]{2,1,0:T(2,128)S(1)} %fusion.1), kind=kOutput, calls=%fused_computation.29 | convolution fusion | flops 1084489728 | bytes 12066816 | tf_op jit(solution)/shard_map/hcqk,khe->hcqe/dot_general | solution.py:61
  113.5 0.0 copy-done.8
  113.5 0.2 multiply_reduce_fusion.1
  113.6 0.0 copy-done
  113.7 0.0 copy-done.9
  113.7 1.8 fusion.6
  115.5 0.0 copy-start.6
  115.5 0.0 copy-start.7
  115.5 0.0 copy-start.2
  115.5 0.0 all-reduce.2.cloned.1.call-update
  115.5 0.0 all-gather.9.cloned.1.call-start
  115.6 0.5 all-gather.9.cloned.1.call-update
  116.1 0.0 all-gather.11.cloned.1.call-start
  116.1 0.5 all-gather.11.cloned.1.call-update
  116.7 0.0 reduce-scatter.2.cloned.1.call-start
  116.7 0.0 copy-done.6
  116.7 0.0 copy-done.7
  116.8 0.1 slice_reduce_fusion.2
  116.8 0.0 copy-start.10
  116.9 35.5 %all-reduce.2.cloned.1.call-done = bf16[256,2048]{1,0:T(8,128)(2,1)} async-done(((bf16[256,2048]{1,0:T(8,128)(2,1)}), bf16[256,2048]{1,0:T(8,128)(2,1)}) %all-reduce.2.cloned.1.call-update) | async-done | bytes 1048592 | tf_op jit(solution)/shard_map/psum | solution.py:74
  152.3 0.0 copy-done.2
  152.3 3.0 convert_add_fusion
  155.3 89.8 %all-gather.9.cloned.1.call-done = bf16[2048,1408]{1,0:T(8,128)(2,1)} async-done(((bf16[256,1408]{1,0:T(8,128)(2,1)}), bf16[2048,1408]{1,0:T(8,128)(2,1)}) %all-gather.9.cloned.1.call-update) | async-done | bytes 5767184 | tf_op jit(solution)/shard_map/all_gather | solution.py:85
  245.1 0.0 copy-done.10
  245.1 4.8 %convolution_convert_fusion.1 = bf16[256,1408]{1,0:T(8,128)(2,1)S(1)} fusion(bf16[2048,1408]{1,0:T(8,128)(2,1)} %all-gather.9.cloned.1.call-done, f32[2048]{0:T(1024)S(1)} %copy-done.10, f32[256]{0:T(256)S(1)} %add_rsqrt_fusion.1, bf16[256,2048]{1,0:T(8,128)(2,1)} %all-reduce.2.cloned.1.call-done, bf16[256,2048]{1,0:T(8,128)(2,1)S(1)} %copy-done.2), kind=kOutput, calls=%fused_computation.10 | convolution fusion | flops 1479901184 | bytes 8594432 | tf_op jit(solution)/shard_map/dot_general | solution.py:83
  249.9 0.0 copy-start.3
  249.9 0.9 copy-done.3
  250.8 1.3 collective-permute-start
  252.1 85.5 %all-gather.11.cloned.1.call-done = bf16[2048,1408]{1,0:T(8,128)(2,1)} async-done(((bf16[256,1408]{1,0:T(8,128)(2,1)}), bf16[2048,1408]{1,0:T(8,128)(2,1)}) %all-gather.11.cloned.1.call-update) | async-done | bytes 5767184 | tf_op jit(solution)/shard_map/all_gather | solution.py:89
  337.6 0.0 copy-start.4
  337.7 4.9 %convolution_convert_fusion = bf16[256,1408]{1,0:T(8,128)(2,1)S(1)} fusion(bf16[2048,1408]{1,0:T(8,128)(2,1)} %all-gather.11.cloned.1.call-done, f32[2048]{0:T(1024)S(1)} %copy-done.10, f32[256]{0:T(256)S(1)} %add_rsqrt_fusion.1, bf16[256,2048]{1,0:T(8,128)(2,1)} %all-reduce.2.cloned.1.call-done, bf16[256,2048]{1,0:T(8,128)(2,1)S(1)} %copy-done.2), kind=kOutput, calls=%fused_computation.9 | convolution fusion | flops 1479901184 | bytes 8594432 | tf_op jit(solution)/shard_map/dot_general | solution.py:88
  342.6 1.5 collective-permute-start.1
  344.0 0.0 collective-permute-done
  344.1 0.0 copy-done.4
  344.1 0.2 maximum_convert_fusion
  344.2 2.7 collective-permute-done.1
  346.9 0.1 maximum_convert_fusion.1
  347.1 6.2 %convolution_convert_fusion.2 = bf16[256,2048]{1,0:T(8,128)(2,1)} fusion(bf16[1408,2048]{1,0:T(8,128)(2,1)} %param.25, f32[258,1408]{1,0:T(8,128)S(1)} %maximum_convert_fusion.1, f32[258,1408]{1,0:T(8,128)S(1)} %maximum_convert_fusion, f32[1408]{0:T(1024)S(1)} %get-tuple-element.9, f32[1408]{0:T(1024)S(1)} %get-tuple-element.10, ...), kind=kOutput, calls=%fused_computation.11 | convolution fusion | flops 1482686464 | bytes 15515648 | tf_op jit(solution)/shard_map/dot_general | solution.py:98
  353.3 0.0 reduce-scatter.2.cloned.1.call-update
  353.4 26.8 %reduce-scatter.2.cloned.1.call-done = bf16[64,2048]{1,0:T(8,128)(2,1)} async-done(((bf16[256,2048]{1,0:T(8,128)(2,1)}), bf16[64,2048]{1,0:T(8,128)(2,1)}) %reduce-scatter.2.cloned.1.call-update) | async-done | bytes 262160 | tf_op jit(solution)/shard_map/reduce_scatter | solution.py:97
  380.2 1.9 add_convert_fusion
  (6 shorter events, 0.0 us)
Async XLA Ops:
  6.5 107.1 %copy-start = (bf16[512,2048]{1,0:T(8,128)(2,1)S(1)}, bf16[512,2048]{1,0:T(8,128)(2,1)}, u32[]{:S(2)}) copy-start(bf16[512,2048]{1,0:T(8,128)(2,1)} %param.19) | copy-start | bytes 6291460
  6.5 50.0 %copy-start.5 = (bf16[256,2,2,128]{3,2,1,0:T(2,128)(2,1)S(1)}, bf16[256,2,2,128]{3,2,1,0:T(2,128)(2,1)}, u32[]{:S(2)}) copy-start(bf16[256,2,2,128]{3,2,1,0:T(2,128)(2,1)} %param.14) | copy-start | bytes 786436
  6.5 50.0 %all-gather.5.cloned.1.call-start = ((), (), s32[]{:S(2)}) async-start(), calls=%async_computation.1 | async-start | bytes 2359296 | tf_op jit(solution)/shard_map/all_gather | solution.py:49
  8.4 99.2 %all-gather.7.cloned.1.call-start = ((), (), s32[]{:S(2)}) async-start(), calls=%async_computation.2 | async-start | bytes 2359296 | tf_op jit(solution)/shard_map/all_gather | solution.py:50
  10.3 142.0 %all-reduce.2.cloned.1.call-start = ((), (), s32[]{:S(2)}) async-start(), calls=%async_computation.3 | async-start | bytes 2097152 | tf_op jit(solution)/shard_map/psum | solution.py:74
  60.0 3.2 copy-start.1
  65.7 47.7 %copy-start.8 = (f32[2]{0:T(128)S(1)}, f32[2]{0:T(128)}, u32[]{:S(2)}) copy-start(f32[2]{0:T(128)} %param.17) | copy-start | bytes 28
  65.7 47.9 %copy-start.9 = (f32[256]{0:T(256)S(1)}, f32[256]{0:T(256)}, u32[]{:S(2)}) copy-start(f32[256]{0:T(256)} %param.18) | copy-start | bytes 3076
  115.5 1.2 copy-start.6
  115.5 1.3 copy-start.7
  115.5 36.9 %copy-start.2 = (bf16[256,2048]{1,0:T(8,128)(2,1)S(1)}, bf16[256,2048]{1,0:T(8,128)(2,1)}, u32[]{:S(2)}) copy-start(bf16[256,2048]{1,0:T(8,128)(2,1)} %param.13) | copy-start | bytes 3145732
  115.5 129.6 %all-gather.9.cloned.1.call-start = ((), (), s32[]{:S(2)}) async-start(), calls=%async_computation.4 | async-start | bytes 6488064 | tf_op jit(solution)/shard_map/all_gather | solution.py:85
  116.1 221.6 %all-gather.11.cloned.1.call-start = ((), (), s32[]{:S(2)}) async-start(), calls=%async_computation.5 | async-start | bytes 6488064 | tf_op jit(solution)/shard_map/all_gather | solution.py:89
  116.7 263.5 %reduce-scatter.2.cloned.1.call-start = ((), (), s32[]{:S(2)}) async-start(), calls=%async_computation.6 | async-start | bytes 1310720 | tf_op jit(solution)/shard_map/reduce_scatter | solution.py:97
  116.8 128.2 %copy-start.10 = (f32[2048]{0:T(1024)S(1)}, f32[2048]{0:T(1024)}, u32[]{:S(2)}) copy-start(f32[2048]{0:T(1024)} %param.20) | copy-start | bytes 24580
  249.9 0.9 copy-start.3
  250.8 93.2 %collective-permute-start = (bf16[2,1408]{1,0:T(2,128)(2,1)S(1)}, bf16[2,1408]{1,0:T(2,128)(2,1)S(1)}, u32[]{:S(2)}, u32[]{:S(2)}) collective-permute-start(bf16[2,1408]{1,0:T(2,128)(2,1)S(1)} %slice.66), channel_id=1, source_target_pairs={{0,4},{4,8},{8,12},{12,16},{16,20},{20,24},{24,28},{1,5},{5,9},{9,... | collective-permute-start | bytes 16904 | tf_op jit(solution)/shard_map/ppermute | solution.py:15
  337.6 6.4 %copy-start.4 = (bf16[256,1408]{1,0:T(8,128)(2,1)S(1)}, bf16[256,1408]{1,0:T(8,128)(2,1)}, u32[]{:S(2)}) copy-start(bf16[256,1408]{1,0:T(8,128)(2,1)} %copy-done.3) | copy-start | bytes 2162692
  342.6 4.4 %collective-permute-start.1 = (bf16[2,1408]{1,0:T(2,128)(2,1)S(1)}, bf16[2,1408]{1,0:T(2,128)(2,1)S(1)}, u32[]{:S(2)}, u32[]{:S(2)}) collective-permute-start(bf16[2,1408]{1,0:T(2,128)(2,1)S(1)} %slice.70), channel_id=1, source_target_pairs={{0,4},{4,8},{8,12},{12,16},{16,20},{20,24},{24,28},{1,5},{5,9},{9,... | collective-permute-start | bytes 16904 | tf_op jit(solution)/shard_map/ppermute | solution.py:15
Sparse Core Ops, SparseCore 0:
  9.5 47.0 all-gather.4
  58.6 48.9 all-gather.6
  115.6 36.6 all-reduce.1
  154.4 90.6 all-gather.8
  247.1 90.4 all-gather.10
  353.5 26.6 reduce-scatter.1
where the time goes:
time: 392 us; the launch traced here: 389 us
  waiting for transfers between devices  329 us (84%)
  matrix products  27 us (7%)
  between operations  13.7 us (3%)
  other arithmetic  8.17 us (2%)
  local copies, waits for them, and re-layouts  7.9 us (2%)
    all_gather x1, waiting for transfers between devices, local(): lax.all_gather(w_gate, 'sp', axis=0, tiled=True)  89.8 us
    all_gather x1, waiting for transfers between devices, local(): lax.all_gather(w_up, 'sp', axis=0, tiled=True)  85.5 us
    all_gather x1, waiting for transfers between devices, local(): key_part = lax.all_gather(key_rows, 'sp', axis=0, tiled=True)  45.8 us
    all_gather x1, waiting for transfers between devices, local(): val_part = lax.all_gather(values, 'sp', axis=0, tiled=True)  41.9 us
    psum x1, waiting for transfers between devices, local(): lax.psum(jnp.einsum('hqe,hed->qd', normed, w_heads, preferred_element_typ...  35.5 us
    reduce_scatter x1, waiting for transfers between devices, local(): lax.psum_scatter(jnp.dot(hidden, w_down, preferred_element_type=jnp.float...  26.8 us
  transfers between devices with their start and end apart: 8, of which 7 were waited for; matrix products, arithmetic and copies ran while one was open for 5% of the time, Pallas kernels for 0%

commit v1 on v0

v1 whole, which is shorter than its diff:
```python
import functools
import math

import jax
import jax.numpy as jnp
from jax import lax
from jax.experimental import pallas as pl
from jax.experimental.pallas import tpu as pltpu
from jax.sharding import PartitionSpec as P

MESH = pl.DeviceIdType.MESH
epsilon = 1e-06
lambda_init = 0.8 - 0.6 * math.exp(-0.3)
bf16 = jnp.bfloat16
f32 = jnp.float32
HALO = 16
UP, DOWN, ACROSS = 0, 1, 2
KV, GATE, UP_A, UP_B = 0, 1, 2, 3


def kernel(
    S, T, heads, dh, dv,
    q_hbm, kv_hbm, res_hbm, wout_hbm, wg_hbm, wu_hbm, wd_hbm,
    lam_ref, sub_ref, norm_ref, cg_ref, cu_ref,
    out_ref,
    q, kv, res, wout, wg, wua, wub, wd,
    m_s, l_s, acc_s, n_s, part, part_in, mid, hn, hb, halo_in, acc_g, acc_u, hid, low, low_in,
    local_sem, send_sem, recv_sem, tp_send, tp_recv, halo_sem, low_send, low_recv,
):
    Z = S // 2
    sp = lax.axis_index("sp")
    tp = lax.axis_index("tp")
    z = lax.div(sp, 2)
    y = lax.rem(sp, 2)
    rows = q.shape[0]
    feat = wg.shape[1]
    half = feat // 2
    D = wout.shape[1]
    own = rows // T
    units = wg.shape[2]
    has_up, has_down = z < Z - 1, z > 0
    has_next, has_prev = sp < S - 1, sp > 0

    def one(flag):
        return flag.astype(jnp.int32)

    def peer(d):
        return lax.rem(tp + d, T)

    target = {UP: sp + 2, DOWN: sp - 2, ACROSS: z * 2 + (1 - y)}
    bufs = {KV: kv, GATE: wg, UP_A: wua, UP_B: wub}

    loads = [
        pltpu.make_async_copy(kv_hbm, kv.at[sp], local_sem.at[0]),
        pltpu.make_async_copy(wg_hbm, wg.at[sp], local_sem.at[1]),
        pltpu.make_async_copy(wu_hbm.at[pl.ds(0, half)], wua.at[sp], local_sem.at[2]),
        pltpu.make_async_copy(wu_hbm.at[pl.ds(half, half)], wub.at[sp], local_sem.at[3]),
        pltpu.make_async_copy(q_hbm, q, local_sem.at[4]),
        pltpu.make_async_copy(wout_hbm, wout, local_sem.at[5]),
        pltpu.make_async_copy(res_hbm, res, local_sem.at[6]),
        pltpu.make_async_copy(wd_hbm, wd, local_sem.at[7]),
    ]
    for c in loads:
        c.start()

    barrier = pltpu.get_barrier_semaphore()

    def greet(device):
        pl.semaphore_signal(barrier, inc=1, device_id=device, device_id_type=MESH)

    pl.when(has_up)(lambda: greet((target[UP], tp)))
    pl.when(has_down)(lambda: greet((target[DOWN], tp)))
    greet((target[ACROSS], tp))
    pl.when(has_next)(lambda: greet((sp + 1, tp)))
    pl.when(has_prev)(lambda: greet((sp - 1, tp)))
    for d in range(1, T):
        greet((sp, peer(d)))
    pl.semaphore_wait(
        barrier, T + one(has_up) + one(has_down) + one(has_next) + one(has_prev)
    )

    def remote(p, blk, way):
        return pltpu.make_async_remote_copy(
            src_ref=bufs[p].at[blk],
            dst_ref=bufs[p].at[blk],
            send_sem=send_sem.at[way, p, blk],
            recv_sem=recv_sem.at[p, blk],
            device_id=(target[way], tp),
            device_id_type=MESH,
        )

    def send(p, blk, way, cond=None):
        if cond is None:
            remote(p, blk, way).start()
        else:
            pl.when(cond)(lambda: remote(p, blk, way).start())

    def sent(p, blk, way):
        remote(p, blk, way).wait_send()

    def arrive(p, blk):
        remote(p, blk, ACROSS).wait_recv()

    loads[0].wait()
    send(KV, sp, UP, has_up)
    send(KV, sp, ACROSS, y == 0)
    for p in (UP_B, GATE, UP_A):
        loads[p].wait()
        send(p, sp, DOWN, has_down)
    loads[4].wait()

    m_s[...] = jnp.full(m_s.shape, -1e30, f32)
    l_s[...] = jnp.zeros(l_s.shape, f32)
    acc_s[...] = jnp.zeros(acc_s.shape, f32)
    scale = 1.0 / math.sqrt(dh)

    def attend(blk):
        row_at = sp * rows + lax.broadcasted_iota(jnp.int32, (rows, rows), 0)
        col_at = blk * rows + lax.broadcasted_iota(jnp.int32, (rows, rows), 1)
        keep = col_at <= row_at
        for h in range(heads):
            v = kv[blk, :, 2 * heads * dh + h * dv : 2 * heads * dh + (h + 1) * dv]
            for c in range(2):
                i = 2 * h + c
                k = kv[blk, :, i * dh : (i + 1) * dh]
                s = lax.dot_general(
                    q[:, i * dh : (i + 1) * dh], k, (((1,), (1,)), ((), ())),
                    preferred_element_type=f32,
                ) * scale
                s = jnp.where(keep, s, -1e30)
                old = m_s[i]
                new = jnp.maximum(old, jnp.max(s, axis=1, keepdims=True))
                e = jnp.where(keep, jnp.exp(s - new), 0.0)
                fade = jnp.exp(old - new)
                m_s[i] = new
                l_s[i] = l_s[i] * fade + jnp.sum(e, axis=1, keepdims=True)
                acc_s[i] = acc_s[i] * fade + jnp.dot(e.astype(bf16), v, preferred_element_type=f32)

    @pl.loop(0, Z)
    def _(r):
        @pl.when(z >= r)
        def _():
            blk = sp - 2 * r

            @pl.when(r > 0)
            def _():
                arrive(KV, blk)
                send(KV, blk, UP, has_up)
                send(KV, blk, ACROSS)

            attend(blk)

    for p in (UP_B, GATE, UP_A):
        send(p, sp, ACROSS)
        send(p, sp, UP, has_up)

    @pl.loop(0, Z)
    def _(r):
        @pl.when((z >= r) & ((r > 0) | (y == 1)))
        def _():
            blk = (z - r) * 2 + (1 - y)
            arrive(KV, blk)
            attend(blk)

    def relay(r):
        @pl.when((r == 0))
        def _():
            b = z * 2 + (1 - y)
            arrive(UP_B, b)
            send(UP_B, b, UP, has_up)
            send(UP_B, b, DOWN, has_down)

        def side(exists, col_z, way, cond):
            @pl.when(exists & (r > 0))
            def _():
                a = col_z * 2 + y
                b = col_z * 2 + (1 - y)
                for p in (UP_B, GATE, UP_A):
                    arrive(p, a)
                    send(p, a, way, cond)
                    if p != UP_B:
                        send(p, a, ACROSS)
                    else:
                        pass
                arrive(UP_B, b)
                send(UP_B, b, way, cond)

        side(z + r < Z, z + r, DOWN, has_down)
        side(z >= r, z - r, UP, has_up)

    first = min(2, Z)

    @pl.loop(0, first)
    def _(r):
        relay(r)

    loads[5].wait()
    for h in range(heads):
        a0 = acc_s[2 * h] / l_s[2 * h]
        a1 = acc_s[2 * h + 1] / l_s[2 * h + 1]
        a = a0 - lam_ref[h] * a1
        ms = jnp.mean(a * a, axis=1, keepdims=True)
        n = a * lax.rsqrt(ms + epsilon) * sub_ref[...] * (1.0 - lambda_init)
        n_s[:, h * dv : (h + 1) * dv] = n.astype(bf16)
    width = min(512, D)
    for c in range(0, D, width):
        part[:, :, c : c + width] = (
            jnp.dot(n_s[...], wout[:, c : c + width], preferred_element_type=f32)
            .astype(bf16)
            .reshape(T, own, width)
        )

    def swap(d, src, dst, k):
        return pltpu.make_async_remote_copy(
            src_ref=src, dst_ref=dst, send_sem=tp_send.at[k, d], recv_sem=tp_recv.at[k, d],
            device_id=(sp, peer(d)), device_id_type=MESH,
        )

    firsts = [swap(d, part.at[peer(d)], part_in.at[d], 0) for d in range(1, T)]
    for c in firsts:
        c.start()
    loads[6].wait()
    total = res[pl.ds(tp * own, own), :].astype(f32) + part[tp].astype(f32)
    for d in range(1, T):
        firsts[d - 1].wait_recv()
        total = total + part_in[d].astype(f32)
    mid[...] = total
    ms = jnp.mean(total * total, axis=1, keepdims=True)
    hn[tp] = (total * lax.rsqrt(ms + epsilon) * norm_ref[...]).astype(bf16)
    seconds = [swap(d, hn.at[tp], hn.at[tp], 1) for d in range(1, T)]
    for c in seconds:
        c.start()
    for d in range(1, T):
        back = lax.rem(tp + T - d, T)
        swap(d, hn.at[back], hn.at[back], 1).wait_recv()

    halo = pltpu.make_async_remote_copy(
        src_ref=hn.at[T - 1, pl.ds(own - HALO, HALO)], dst_ref=halo_in,
        send_sem=halo_sem.at[0], recv_sem=halo_sem.at[1],
        device_id=(sp + 1, tp), device_id_type=MESH,
    )
    pl.when(has_next)(halo.start)

    @pl.loop(first, Z)
    def _(r):
        relay(r)

    pl.when(has_prev)(halo.wait_recv)

    @pl.when(jnp.logical_not(has_prev))
    def _():
        halo_in[...] = jnp.zeros(halo_in.shape, bf16)

    for j in range(S):
        hb[j, :HALO, :] = halo_in[:, j * feat : (j + 1) * feat]
        hb[j, HALO:, :] = hn[:, :, j * feat : (j + 1) * feat].reshape(rows, feat)

    acc_g[...] = jnp.zeros(acc_g.shape, f32)
    acc_u[...] = jnp.zeros(acc_u.shape, f32)

    def mul(blk):
        acc_g[...] += jnp.dot(hb[blk], wg[blk], preferred_element_type=f32)
        acc_u[...] += jnp.dot(hb[blk, :, :half], wua[blk], preferred_element_type=f32)
        acc_u[...] += jnp.dot(hb[blk, :, half:], wub[blk], preferred_element_type=f32)

    @pl.loop(0, Z)
    def _(k):
        mul(2 * k + y)

    def take(blk):
        arrive(GATE, blk)
        arrive(UP_A, blk)
        mul(blk)

    @pl.loop(0, Z)
    def _(r):
        pl.when((z + r < Z) & (r > 0))(lambda: take((z + r) * 2 + 1 - y))
        pl.when(z >= r)(lambda: take((z - r) * 2 + 1 - y))

    for c in range(0, units, 128):
        cols = slice(c, c + 128)
        g = acc_g[:, cols].astype(bf16).astype(f32)
        u = acc_u[:, cols].astype(bf16).astype(f32)

        def mix(x, taps):
            out = taps[0:1, cols] * x[HALO - 2 : HALO - 2 + rows]
            out = out + taps[1:2, cols] * x[HALO - 1 : HALO - 1 + rows]
            return out + taps[2:3, cols] * x[HALO:]

        gm, um = mix(g, cg_ref), mix(u, cu_ref)
        hid[:, cols] = (gm / (1.0 + jnp.exp(-gm)) * um).astype(bf16)

    loads[7].wait()
    chunks, cw = low.shape[0], low.shape[3]
    lows = []
    for c in range(chunks):
        low[c] = (
            jnp.dot(hid[...], wd[:, c * cw : (c + 1) * cw], preferred_element_type=f32)
            .astype(bf16)
            .reshape(T, own, cw)
        )
        for d in range(1, T):
            copy = pltpu.make_async_remote_copy(
                src_ref=low.at[c, peer(d)], dst_ref=low_in.at[c, d],
                send_sem=low_send.at[c, d], recv_sem=low_recv.at[c, d],
                device_id=(sp, peer(d)), device_id_type=MESH,
            )
            copy.start()
            lows.append(copy)

    @pl.loop(0, Z)
    def _(k):
        a = 2 * k + y
        b = 2 * k + 1 - y
        pl.when(has_up & (k <= z))(lambda: sent(KV, a, UP))
        pl.when((k < z) | ((k == z) & (y == 0)))(lambda: sent(KV, a, ACROSS))
        for p in (GATE, UP_A):
            sent(p, a, ACROSS)
        pl.when(k == z)(lambda: sent(UP_B, a, ACROSS))
        for p, blk in ((GATE, a), (UP_A, a), (UP_B, a), (UP_B, b)):
            pl.when(has_up & (k <= z))(functools.partial(sent, p, blk, UP))
            pl.when(has_down & (k >= z))(functools.partial(sent, p, blk, DOWN))

    for c in firsts + seconds:
        c.wait_send()
    pl.when(has_next)(halo.wait_send)

    for c in range(chunks):
        cols = slice(c * cw, (c + 1) * cw)
        total = mid[:, cols] + low[c, tp].astype(f32)
        for d in range(1, T):
            lows[c * (T - 1) + d - 1].wait_recv()
            total = total + low_in[c, d].astype(f32)
        out_ref[:, cols] = total.astype(bf16)
    for c in lows:
        c.wait_send()


def local(
    S, T,
    residual, queries, key_rows, values, lambda_head, sub_gain, w_out, norm_gain,
    w_gate, w_up, conv_gate, conv_up, w_down,
):
    rows, heads, maps, dh = queries.shape
    dv = values.shape[2]
    feat, units = w_gate.shape
    D = w_out.shape[1]
    own = rows // T
    half = feat // 2
    q = queries.reshape(rows, heads * maps * dh)
    kv = jnp.concatenate(
        [key_rows.reshape(rows, heads * maps * dh), values.reshape(rows, heads * dv)], axis=1
    )
    kvw = kv.shape[1]
    cw = math.gcd(D, 512)
    chunks = D // cw
    hbm = pl.BlockSpec(memory_space=pl.ANY)
    vmem = pl.BlockSpec(memory_space=pltpu.VMEM)
    smem = pl.BlockSpec(memory_space=pltpu.SMEM)
    padded = rows + HALO
    V = pltpu.VMEM
    dma = pltpu.SemaphoreType.DMA
    return pl.pallas_call(
        functools.partial(kernel, S, T, heads, dh, dv),
        out_shape=jax.ShapeDtypeStruct((own, D), bf16),
        in_specs=[hbm] * 7 + [smem] + [vmem] * 4,
        out_specs=vmem,
        scratch_shapes=[
            V((rows, q.shape[1]), bf16),
            V((S, rows, kvw), bf16),
            V((rows, D), bf16),
            V(w_out.shape, bf16),
            V((S, feat, units), bf16),
            V((S, half, units), bf16),
            V((S, half, units), bf16),
            V(w_down.shape, bf16),
            V((2 * heads, rows, 1), f32),
            V((2 * heads, rows, 1), f32),
            V((2 * heads, rows, dv), f32),
            V((rows, heads * dv), bf16),
            V((T, own, D), bf16),
            V((T, own, D), bf16),
            V((own, D), f32),
            V((T, own, D), bf16),
            V((S, padded, feat), bf16),
            V((HALO, D), bf16),
            V((padded, units), f32),
            V((padded, units), f32),
            V((rows, units), bf16),
            V((chunks, T, own, cw), bf16),
            V((chunks, T, own, cw), bf16),
            dma((8,)),
            dma((3, 4, S)),
            dma((4, S)),
            dma((2, T)),
            dma((2, T)),
            dma((2,)),
            dma((chunks, T)),
            dma((chunks, T)),
        ],
        compiler_params=pltpu.CompilerParams(
            collective_id=0, has_side_effects=True, vmem_limit_bytes=64000000
        ),
    )(
        q, kv, residual, w_out, w_gate, w_up, w_down, lambda_head,
        sub_gain.reshape(1, -1), norm_gain.reshape(1, -1), conv_gate, conv_up,
    )


def solution(mesh):
    placed = (
        P("sp", None),
        P("sp", "tp", None, None),
        P("sp", "tp", None, None),
        P("sp", "tp", None),
        P("tp"),
        P(),
        P("tp", None),
        P(),
        P("sp", "tp"),
        P("sp", "tp"),
        P(None, "tp"),
        P(None, "tp"),
        P("tp", None),
    )
    return jax.shard_map(
        functools.partial(local, mesh.shape["sp"], mesh.shape["tp"]),
        mesh=mesh, in_specs=placed, out_specs=P(("sp", "tp"), None), check_vma=False,
    )
```

time: 392 us -> 183 us (0.47)
  waiting for transfers between devices: 329 us -> 0 us
  Pallas kernels: 0 us -> 176 us
  matrix products: 27 us -> 0 us
  between operations: 13.7 us -> 0.02 us
  other arithmetic: 8.17 us -> 0.86 us
    all_gather x4 -> x0, waiting for transfers between devices: 263 us -> none  [the longest x1 89.8 us: local(): lax.all_gather(w_gate, 'sp', axis=0, tiled=True)]
    pallas_call x0 -> x1, Pallas kernels: none -> 176 us  [local(): pl.pallas_call(functools.partial(kernel, S, T, heads, dh, dv), out_shape=...]
    psum x1 -> x0, waiting for transfers between devices: 35.5 us -> none  [local(): lax.psum(jnp.einsum('hqe,hed->qd', normed, w_heads, preferred_element_typ...]
    dot_general x6 -> x0, matrix products: 27 us -> none  [the longest x1 6.24 us: local(): jnp.dot(hidden, w_down, preferred_element_type=jnp.float32)]
    reduce_scatter x1 -> x0, waiting for transfers between devices: 26.8 us -> none  [local(): lax.psum_scatter(jnp.dot(hidden, w_down, preferred_element_type=jnp.float...]
    unnamed x24 -> x2, local copies, waits for them, and re-layouts: 7.78 us -> 2.65 us
  transfers between devices with their start and end apart: 8 -> 0, of which waited for: 7 -> 0; matrix products, arithmetic and copies ran while one was open for 5% -> 0% of each run, Pallas kernels for 0% -> 0%
where the time goes in v1:
time: 183 us; the launch traced here: 182 us
  Pallas kernels  176 us (96%)
  local copies, waits for them, and re-layouts  5.46 us (3%)
    pallas_call x1, Pallas kernels, local(): pl.pallas_call(functools.partial(kernel, S, T, heads, dh, dv), out_shape=...  176 us

profile of v1, /device:TPU:31, one launch (start us, length us, event | category | flops | bytes accessed | tf_op | source)
XLA Modules:
  0.0 182.3 jit_solution(10499258127196559588)
XLA Ops:
  0.0 1.0 copy.14
  1.0 1.1 reshape.16
  2.0 0.9 pad_maximum_fusion.kv_hbm
  2.9 1.8 reshape.15.q_hbm
  4.7 175.9 %shard_map.127 = bf16[64,2048]{1,0:T(8,128)(2,1)} custom-call(bf16[256,512]{1,0:T(8,128)(2,1)} %reshape.15.q_hbm, bf16[256,1024]{1,0:T(8,128)(2,1)} %pad_maximum_fusion.kv_hbm, bf16[256,2048]{1,0:T(8,128)(2,1)} %res_hbm.1, bf16[512,2048]{1,0:T(8,128)(2,1)} %wout_hbm.1, bf16[256,1408]{1,0:T(8,128)(2,1)} %wg_hbm.1, bf16[256,1408]{1,0:T(8,128)(2,1)} %wu_hbm.1, ...), custom_call_target="tpu_custom_call" | custom-call | tf_op jit(solution)/shard_map/pallas_call | solution.py:363
  180.6 1.7 copy.16

commit v2 on v1

--- a/solution.py
+++ b/solution.py
@@ -24,17 +24,20 @@
     lam_ref, sub_ref, norm_ref, cg_ref, cu_ref,
     out_ref,
     q, kv, res, wout, wg, wua, wub, wd,
-    m_s, l_s, acc_s, n_s, part, part_in, mid, hn, hb, halo_in, acc_g, acc_u, hid, low, low_in,
-    local_sem, send_sem, recv_sem, tp_send, tp_recv, halo_sem, low_send, low_recv,
+    m_s, l_s, acc_s, n_own, n_in, part, part_in, mid, hn, hb, halo_in, acc_g, acc_u, hid, low, low_in,
+    local_sem, pair_sem, send_sem, recv_sem, tp_send, tp_recv, halo_sem, low_send, low_recv,
 ):
     Z = S // 2
     sp = lax.axis_index("sp")
     tp = lax.axis_index("tp")
     z = lax.div(sp, 2)
     y = lax.rem(sp, 2)
-    rows = q.shape[0]
+    rows = q.shape[1]
     feat = wg.shape[1]
-    half = feat // 2
+    tail = wub.shape[2]
+    split = wua.shape[2]
+    hh = heads // 2
+    kw = 2 * hh * dh
     D = wout.shape[1]
     own = rows // T
     units = wg.shape[2]
@@ -51,11 +54,11 @@
     bufs = {KV: kv, GATE: wg, UP_A: wua, UP_B: wub}
 
     loads = [
-        pltpu.make_async_copy(kv_hbm, kv.at[sp], local_sem.at[0]),
+        pltpu.make_async_copy(kv_hbm.at[y], kv.at[sp], local_sem.at[0]),
         pltpu.make_async_copy(wg_hbm, wg.at[sp], local_sem.at[1]),
-        pltpu.make_async_copy(wu_hbm.at[pl.ds(0, half)], wua.at[sp], local_sem.at[2]),
-        pltpu.make_async_copy(wu_hbm.at[pl.ds(half, half)], wub.at[sp], local_sem.at[3]),
-        pltpu.make_async_copy(q_hbm, q, local_sem.at[4]),
+        pltpu.make_async_copy(wu_hbm.at[:, pl.ds(0, split)], wua.at[sp], local_sem.at[2]),
+        pltpu.make_async_copy(wu_hbm.at[:, pl.ds(split, tail)], wub.at[sp], local_sem.at[3]),
+        pltpu.make_async_copy(q_hbm.at[y], q.at[y], local_sem.at[4]),
         pltpu.make_async_copy(wout_hbm, wout, local_sem.at[5]),
         pltpu.make_async_copy(res_hbm, res, local_sem.at[6]),
         pltpu.make_async_copy(wd_hbm, wd, local_sem.at[7]),
@@ -101,12 +104,27 @@
     def arrive(p, blk):
         remote(p, blk, ACROSS).wait_recv()
 
+    other = 1 - y
+    across = (target[ACROSS], tp)
+
+    def pair(src, dst, k):
+        return pltpu.make_async_remote_copy(
+            src_ref=src, dst_ref=dst, send_sem=pair_sem.at[0, k], recv_sem=pair_sem.at[1, k],
+            device_id=across, device_id_type=MESH,
+        )
+
+    kv_swap = pair(kv_hbm.at[other], kv.at[sp], 0)
+    q_swap = pair(q_hbm.at[other], q.at[y], 1)
+    kv_got = pair(kv_hbm.at[other], kv.at[target[ACROSS]], 0)
+    q_got = pair(q_hbm.at[other], q.at[other], 1)
+    kv_swap.start()
+    q_swap.start()
     loads[0].wait()
     send(KV, sp, UP, has_up)
-    send(KV, sp, ACROSS, y == 0)
     for p in (UP_B, GATE, UP_A):
         loads[p].wait()
         send(p, sp, DOWN, has_down)
+        send(p, sp, ACROSS)
     loads[4].wait()
 
     m_s[...] = jnp.full(m_s.shape, -1e30, f32)
@@ -114,53 +132,62 @@
     acc_s[...] = jnp.zeros(acc_s.shape, f32)
     scale = 1.0 / math.sqrt(dh)
 
-    def attend(blk):
-        row_at = sp * rows + lax.broadcasted_iota(jnp.int32, (rows, rows), 0)
+    def attend(yy, blk):
+        row_at = (z * 2 + yy) * rows + lax.broadcasted_iota(jnp.int32, (rows, rows), 0)
         col_at = blk * rows + lax.broadcasted_iota(jnp.int32, (rows, rows), 1)
         keep = col_at <= row_at
-        for h in range(heads):
-            v = kv[blk, :, 2 * heads * dh + h * dv : 2 * heads * dh + (h + 1) * dv]
+        for h in range(hh):
+            v = kv[blk, :, kw + h * dv : kw + (h + 1) * dv]
             for c in range(2):
                 i = 2 * h + c
                 k = kv[blk, :, i * dh : (i + 1) * dh]
                 s = lax.dot_general(
-                    q[:, i * dh : (i + 1) * dh], k, (((1,), (1,)), ((), ())),
+                    q[yy, :, i * dh : (i + 1) * dh], k, (((1,), (1,)), ((), ())),
                     preferred_element_type=f32,
                 ) * scale
                 s = jnp.where(keep, s, -1e30)
-                old = m_s[i]
+                old = m_s[yy, i]
                 new = jnp.maximum(old, jnp.max(s, axis=1, keepdims=True))
                 e = jnp.where(keep, jnp.exp(s - new), 0.0)
                 fade = jnp.exp(old - new)
-                m_s[i] = new
-                l_s[i] = l_s[i] * fade + jnp.sum(e, axis=1, keepdims=True)
-                acc_s[i] = acc_s[i] * fade + jnp.dot(e.astype(bf16), v, preferred_element_type=f32)
+                m_s[yy, i] = new
+                l_s[yy, i] = l_s[yy, i] * fade + jnp.sum(e, axis=1, keepdims=True)
+                acc_s[yy, i] = acc_s[yy, i] * fade + jnp.dot(
+                    e.astype(bf16), v, preferred_element_type=f32
+                )
+
+    kv_got.wait_recv()
+    q_got.wait_recv()
+    send(KV, target[ACROSS], UP, has_up)
 
     @pl.loop(0, Z)
     def _(r):
         @pl.when(z >= r)
         def _():
-            blk = sp - 2 * r
-
             @pl.when(r > 0)
             def _():
-                arrive(KV, blk)
-                send(KV, blk, UP, has_up)
-                send(KV, blk, ACROSS)
-
-            attend(blk)
+                for blk in (sp - 2 * r, target[ACROSS] - 2 * r):
+                    arrive(KV, blk)
+                    send(KV, blk, UP, has_up)
+
+            @pl.loop(0, 4)
+            def _(i):
+                yy, c = lax.div(i, 2), lax.rem(i, 2)
+                pl.when((r > 0) | (yy >= c))(lambda: attend(yy, (z - r) * 2 + c))
 
     for p in (UP_B, GATE, UP_A):
-        send(p, sp, ACROSS)
         send(p, sp, UP, has_up)
 
-    @pl.loop(0, Z)
-    def _(r):
-        @pl.when((z >= r) & ((r > 0) | (y == 1)))
-        def _():
-            blk = (z - r) * 2 + (1 - y)
-            arrive(KV, blk)
-            attend(blk)
+    for yy in range(2):
+        for h in range(hh):
+            a0 = acc_s[yy, 2 * h] / l_s[yy, 2 * h]
+            a1 = acc_s[yy, 2 * h + 1] / l_s[yy, 2 * h + 1]
+            a = a0 - lam_ref[y * hh + h] * a1
+            ms = jnp.mean(a * a, axis=1, keepdims=True)
+            n = a * lax.rsqrt(ms + epsilon) * sub_ref[...] * (1.0 - lambda_init)
+            n_own[yy, :, h * dv : (h + 1) * dv] = n.astype(bf16)
+    n_swap = pair(n_own.at[other], n_in, 2)
+    n_swap.start()
 
     def relay(r):
         @pl.when((r == 0))
@@ -175,13 +202,11 @@
             def _():
                 a = col_z * 2 + y
                 b = col_z * 2 + (1 - y)
-                for p in (UP_B, GATE, UP_A):
+                for p in (GATE, UP_A, UP_B):
                     arrive(p, a)
                     send(p, a, way, cond)
                     if p != UP_B:
                         send(p, a, ACROSS)
-                    else:
-                        pass
                 arrive(UP_B, b)
                 send(UP_B, b, way, cond)
 
@@ -195,17 +220,16 @@
         relay(r)
 
     loads[5].wait()
-    for h in range(heads):
-        a0 = acc_s[2 * h] / l_s[2 * h]
-        a1 = acc_s[2 * h + 1] / l_s[2 * h + 1]
-        a = a0 - lam_ref[h] * a1
-        ms = jnp.mean(a * a, axis=1, keepdims=True)
-        n = a * lax.rsqrt(ms + epsilon) * sub_ref[...] * (1.0 - lambda_init)
-        n_s[:, h * dv : (h + 1) * dv] = n.astype(bf16)
+    n_swap.wait_recv()
     width = min(512, D)
+    hw = hh * dv
     for c in range(0, D, width):
-        part[:, :, c : c + width] = (
-            jnp.dot(n_s[...], wout[:, c : c + width], preferred_element_type=f32)
+        cols = slice(c, c + width)
+        part[:, :, cols] = (
+            (
+                jnp.dot(n_own[y], wout[pl.ds(y * hw, hw), cols], preferred_element_type=f32)
+                + jnp.dot(n_in[...], wout[pl.ds(other * hw, hw), cols], preferred_element_type=f32)
+            )
             .astype(bf16)
             .reshape(T, own, width)
         )
@@ -260,8 +284,8 @@
 
     def mul(blk):
         acc_g[...] += jnp.dot(hb[blk], wg[blk], preferred_element_type=f32)
-        acc_u[...] += jnp.dot(hb[blk, :, :half], wua[blk], preferred_element_type=f32)
-        acc_u[...] += jnp.dot(hb[blk, :, half:], wub[blk], preferred_element_type=f32)
+        acc_u[:, :split] += jnp.dot(hb[blk], wua[blk], preferred_element_type=f32)
+        acc_u[:, split:] += jnp.dot(hb[blk], wub[blk], preferred_element_type=f32)
 
     @pl.loop(0, Z)
     def _(k):
@@ -312,16 +336,15 @@
     def _(k):
         a = 2 * k + y
         b = 2 * k + 1 - y
-        pl.when(has_up & (k <= z))(lambda: sent(KV, a, UP))
-        pl.when((k < z) | ((k == z) & (y == 0)))(lambda: sent(KV, a, ACROSS))
         for p in (GATE, UP_A):
             sent(p, a, ACROSS)
         pl.when(k == z)(lambda: sent(UP_B, a, ACROSS))
-        for p, blk in ((GATE, a), (UP_A, a), (UP_B, a), (UP_B, b)):
+        for p, blk in ((KV, a), (KV, b), (GATE, a), (UP_A, a), (UP_B, a), (UP_B, b)):
             pl.when(has_up & (k <= z))(functools.partial(sent, p, blk, UP))
-            pl.when(has_down & (k >= z))(functools.partial(sent, p, blk, DOWN))
-
-    for c in firsts + seconds:
+            if p != KV:
+                pl.when(has_down & (k >= z))(functools.partial(sent, p, blk, DOWN))
+
+    for c in firsts + seconds + [kv_swap, q_swap, n_swap]:
         c.wait_send()
     pl.when(has_next)(halo.wait_send)
 
@@ -346,12 +369,13 @@
     feat, units = w_gate.shape
     D = w_out.shape[1]
     own = rows // T
-    half = feat // 2
-    q = queries.reshape(rows, heads * maps * dh)
+    tail = 3 * math.gcd(units, 128)
+    hh = heads // 2
+    q = queries.reshape(rows, 2, hh * maps * dh).swapaxes(0, 1)
     kv = jnp.concatenate(
-        [key_rows.reshape(rows, heads * maps * dh), values.reshape(rows, heads * dv)], axis=1
-    )
-    kvw = kv.shape[1]
+        [key_rows.reshape(rows, 2, hh * maps * dh), values.reshape(rows, 2, hh * dv)], axis=2
+    ).swapaxes(0, 1)
+    kvw = kv.shape[2]
     cw = math.gcd(D, 512)
     chunks = D // cw
     hbm = pl.BlockSpec(memory_space=pl.ANY)
@@ -366,18 +390,19 @@
         in_specs=[hbm] * 7 + [smem] + [vmem] * 4,
         out_specs=vmem,
         scratch_shapes=[
-            V((rows, q.shape[1]), bf16),
+            V(q.shape, bf16),
             V((S, rows, kvw), bf16),
             V((rows, D), bf16),
             V(w_out.shape, bf16),
             V((S, feat, units), bf16),
-            V((S, half, units), bf16),
-            V((S, half, units), bf16),
+            V((S, feat, units - tail), bf16),
+            V((S, feat, tail), bf16),
             V(w_down.shape, bf16),
-            V((2 * heads, rows, 1), f32),
-            V((2 * heads, rows, 1), f32),
-            V((2 * heads, rows, dv), f32),
-            V((rows, heads * dv), bf16),
+            V((2, 2 * hh, rows, 1), f32),
+            V((2, 2 * hh, rows, 1), f32),
+            V((2, 2 * hh, rows, dv), f32),
+            V((2, rows, hh * dv), bf16),
+            V((rows, hh * dv), bf16),
             V((T, own, D), bf16),
             V((T, own, D), bf16),
             V((own, D), f32),
@@ -390,6 +415,7 @@
             V((chunks, T, own, cw), bf16),
             V((chunks, T, own, cw), bf16),
             dma((8,)),
+            dma((2, 3)),
             dma((3, 4, S)),
             dma((4, S)),
             dma((2, T)),

time: 183 us -> 176 us (0.962)
  Pallas kernels: 176 us -> 169 us
    pallas_call x1, Pallas kernels: 176 us -> 169 us  [local(): pl.pallas_call(functools.partial(kernel, S, T, heads, dh, dv), out_shape=...]
where the time goes in v2:
time: 176 us; the launch traced here: 175 us
  Pallas kernels  169 us (96%)
  local copies, waits for them, and re-layouts  5.65 us (3%)
    pallas_call x1, Pallas kernels, local(): pl.pallas_call(functools.partial(kernel, S, T, heads, dh, dv), out_shape=...  169 us

profile of v2, /device:TPU:31, one launch (start us, length us, event | category | flops | bytes accessed | tf_op | source)
XLA Modules:
  0.0 175.4 jit_solution(18121421126003016947)
XLA Ops:
  0.0 1.1 reshape.17
  1.2 1.0 copy.16
  2.1 0.8 maximum_bitcast_fusion.kv_hbm
  3.0 1.1 reshape.16
  4.1 0.7 copy.20
  4.8 168.9 %shard_map.127 = bf16[64,2048]{1,0:T(8,128)(2,1)} custom-call(bf16[2,256,256]{2,1,0:T(8,128)(2,1)} %bitcast.7, bf16[2,256,512]{2,1,0:T(8,128)(2,1)} %maximum_bitcast_fusion.kv_hbm, bf16[256,2048]{1,0:T(8,128)(2,1)} %res_hbm.1, bf16[512,2048]{1,0:T(8,128)(2,1)} %wout_hbm.1, bf16[256,1408]{1,0:T(8,128)(2,1)} %wg_hbm.1, bf16[256,1408]{1,0:T(8,128)(2,1)} %wu_hbm.1, ...), custom_call_target="tpu_custom_call" | custom-call | tf_op jit(solution)/shard_map/pallas_call | solution.py:387
  173.7 1.7 copy.22
  (1 shorter events, 0.0 us)
